TPU v7x, 32 devices: a whole 2x2x4 slice. The times are simulated.
32 devices in a mesh: gr: 2 (over x), fs: 4 (over z), tp: 4 (over y, core).
Axes of the slice: x: 2, y: 2, z: 4, core: 2. Of those that a mesh axis runs over, the one named last changes fastest.
Arguments:
- tokens: bfloat16 [1536, 4096], P(('gr', 'fs'), 'tp'), may hold values from -6 to 6
- route_ids: int32 [1536, 2], P(('gr', 'fs')), may hold values from 0 to 3, all different within a row; in each aligned block of 192 rows (0 to 191, 192 to 383, ...) at most 192 rows name the same one
- route_logits: float32 [1536, 2], P(('gr', 'fs')), may hold values from -6 to 6
- gain: float32 [4096], P(('gr', 'fs')), may hold values from 0.1 to 1.9
- gate_master: float32 [4, 4096, 2048], P(None, ('gr', 'fs'), 'tp'), may hold values from -6 to 6
- up_master: float32 [4, 4096, 2048], P(None, ('gr', 'fs'), 'tp'), may hold values from -6 to 6
- down_master: float32 [4, 2048, 4096], P(None, ('gr', 'fs'), 'tp'), may hold values from -6 to 6
Outputs:
- gate_weight: bfloat16 [4, 4096, 2048], P('fs', None, 'tp')
- up_weight: bfloat16 [4, 4096, 2048], P('fs', None, 'tp')
- down_weight: bfloat16 [4, 2048, 4096], P('fs', 'tp')
- mixed_out: bfloat16 [1536, 4096], P(('gr', 'fs'), 'tp')
Inputs may be any that keep to these rules, and one draw needn't show every extreme that they name: `route_ids`: each row names 2 different experts; among the rows of one device no expert is named by more than 192 rows, a bound that some block reaches.
All inputs are finite; a program needn't handle non-finite values.
Results may differ from a plain program's by a relative error of at most 0.015.
Values may be sent and summed in bfloat16 or wider, within the bound.
A program may use at most 128 MiB of HBM per device.

v0:
```python
import jax
import jax.numpy as jnp
from jax import lax
from jax.sharding import PartitionSpec as P

EPS = 1e-06


def slot_tables(route_ids, experts, capacity):
    assign_count = route_ids.shape[0] * route_ids.shape[1]
    flattened = route_ids.reshape(assign_count)
    onehot = (flattened[:, None] == jnp.arange(experts, dtype=jnp.int32)[None, :]).astype(jnp.int32)
    earlier = jnp.cumsum(onehot, axis=0) - onehot
    slot_rank = jnp.sum(earlier * onehot, axis=1)
    position = flattened * capacity + slot_rank
    source = (
        jnp.full((experts * capacity,), assign_count, jnp.int32)
        .at[position]
        .set(jnp.arange(assign_count, dtype=jnp.int32))
    )
    return (position, source)


def fill_slots(normed, source, top_count, experts, capacity):
    token_total = normed.shape[0]
    padded = jnp.concatenate([normed, jnp.zeros((1, normed.shape[1]), normed.dtype)], axis=0)
    token_index = jnp.where(source < token_total * top_count, source // top_count, token_total)
    return padded[token_index].reshape(experts, capacity, normed.shape[1])


def body(tokens, route_ids, route_logits, gain, gate_master, up_master, down_master):
    experts = gate_master.shape[0]
    token_total = route_ids.shape[0]
    top_count = route_ids.shape[1]
    capacity = 2 * token_total * top_count // experts
    row_gain = gain[None, :, None]
    gate_cast = (gate_master * row_gain).astype(jnp.bfloat16)
    up_cast = (up_master * row_gain).astype(jnp.bfloat16)
    down_cast = down_master.astype(jnp.bfloat16)
    owner_gate, owner_up, owner_down = (
        lax.all_to_all(gate_cast, "fs", split_axis=0, concat_axis=1, tiled=True),
        lax.all_to_all(up_cast, "fs", split_axis=0, concat_axis=1, tiled=True),
        lax.all_to_all(down_cast, "fs", split_axis=0, concat_axis=1, tiled=True),
    )
    gate_full, up_full, down_full = (
        lax.all_gather(owner_gate, "gr", axis=1, tiled=True),
        lax.all_gather(owner_up, "gr", axis=1, tiled=True),
        lax.all_gather(owner_down, "gr", axis=1, tiled=True),
    )
    down_rows = lax.all_to_all(down_full, "tp", split_axis=1, concat_axis=2, tiled=True)
    sigmoid_vals = jax.nn.sigmoid(route_logits)
    shares = sigmoid_vals / jnp.sum(sigmoid_vals, axis=1, keepdims=True)
    position, source = slot_tables(route_ids, experts, capacity)
    model_width = gate_full.shape[1]
    full_rows = lax.all_gather(tokens, "tp", axis=1, tiled=True)
    float_rows = full_rows.astype(jnp.float32)
    normed = (
        float_rows * lax.rsqrt(jnp.mean(float_rows * float_rows, axis=1, keepdims=True) + EPS)
    ).astype(jnp.bfloat16)
    buffer = fill_slots(normed, source, top_count, experts, capacity)
    arrived = lax.all_to_all(buffer, "fs", split_axis=0, concat_axis=1, tiled=True)
    gate_sum = jnp.einsum("erd,edf->erf", arrived, gate_full, preferred_element_type=jnp.float32)
    up_sum = jnp.einsum("erd,edf->erf", arrived, up_full, preferred_element_type=jnp.float32)
    scale_in = model_width ** (-0.5)
    hidden = (jax.nn.silu(gate_sum * scale_in) * (up_sum * scale_in)).astype(jnp.bfloat16)
    partial_value = jnp.einsum(
        "erf,efd->erd", hidden, down_rows, preferred_element_type=jnp.float32
    )
    summed = lax.psum_scatter(
        partial_value.astype(jnp.bfloat16), "tp", scatter_dimension=2, tiled=True
    ).astype(jnp.float32)
    expert_out = (summed * down_full.shape[1] ** (-0.5)).astype(jnp.bfloat16)
    returned = lax.all_to_all(expert_out, "fs", split_axis=1, concat_axis=0, tiled=True)
    picked = returned.reshape(experts * capacity, returned.shape[2])[position].astype(jnp.float32)
    weighted = picked * shares.reshape(token_total * top_count)[:, None]
    mixed_out = jnp.sum(weighted.reshape(token_total, top_count, returned.shape[2]), axis=1).astype(
        jnp.bfloat16
    )
    return (gate_full, up_full, down_rows, mixed_out)


def solution(mesh):
    in_specs = (
        P(("gr", "fs"), "tp"),
        P(("gr", "fs"), None),
        P(("gr", "fs"), None),
        P(("gr", "fs")),
        P(None, ("gr", "fs"), "tp"),
        P(None, ("gr", "fs"), "tp"),
        P(None, ("gr", "fs"), "tp"),
    )
    out_specs = (
        P("fs", None, "tp"),
        P("fs", None, "tp"),
        P("fs", "tp", None),
        P(("gr", "fs"), "tp"),
    )
    return jax.shard_map(body, mesh=mesh, in_specs=in_specs, out_specs=out_specs, check_vma=False)
```

profile of v0, /device:TPU:0, one launch (start us, length us, event | category | flops | bytes accessed | tf_op | source)
XLA Modules:
  0.0 530.9 jit_solution(6687284316396528108)
XLA Ops:
  7.2 3.8 convert_element_type.50
  11.0 6.5 %all-to-all-start.2 = ((bf16[4,256,1024]{2,1,0:T(8,128)(2,1)}), bf16[4,256,1024]{2,1,0:T(8,128)(2,1)S(1)}, u32[]{:S(2)}, u32[]{:S(2)}) async-start(bf16[4,256,1024]{2,1,0:T(8,128)(2,1)} %convert_element_type.50), calls=%async_computation.2 | async-start | bytes 4194304 | tf_op jit(solution)/shard_map/all_to_all | solution.py:43
  17.5 6.8 %multiply_convert_fusion = (bf16[4,512,512]{2,1,0:T(8,128)(2,1)}, bf16[4,512,512]{2,1,0:T(8,128)(2,1)}) fusion(f32[4,512,512]{2,1,0:T(8,128)} %param.12, f32[512]{0:T(512)S(1)} %copy-done.5, f32[4,512,512]{2,1,0:T(8,128)} %param.11), kind=kLoop, calls=%fused_computation.9 | loop fusion | flops 4194304 | bytes 12584960 | tf_op jit(solution)/shard_map/convert_element_type | solution.py:38
  24.2 41.4 %all-to-all-done.2 = bf16[4,256,1024]{2,1,0:T(8,128)(2,1)S(1)} async-done(((bf16[4,256,1024]{2,1,0:T(8,128)(2,1)}), bf16[4,256,1024]{2,1,0:T(8,128)(2,1)S(1)}, u32[]{:S(2)}, u32[]{:S(2)}) %all-to-all-start.2) | async-done | bytes 2097184 | tf_op jit(solution)/shard_map/all_to_all | solution.py:43
  65.7 1.3 copy-done.1
  67.0 3.6 all-to-all-start.1
  70.7 0.7 all-gather.9.cloned.1.call-update
  71.4 47.0 %all-to-all-done.1 = bf16[4,512,512]{2,1,0:T(8,128)(2,1)S(1)} async-done(((bf16[4,512,512]{2,1,0:T(8,128)(2,1)}), bf16[4,512,512]{2,1,0:T(8,128)(2,1)S(1)}, u32[]{:S(2)}, u32[]{:S(2)}) %all-to-all-start.1) | async-done | bytes 2097184 | tf_op jit(solution)/shard_map/all_to_all | solution.py:42
  118.3 4.5 all-to-all-start
  122.8 0.7 all-gather.11.cloned.1.call-update
  123.6 8.2 %all-gather.9.cloned.1.call-done = bf16[1,2048,1024]{2,1,0:T(8,128)(2,1)} async-done(((bf16[1,1024,1024]{2,1,0:T(8,128)(2,1)}), bf16[1,2048,1024]{2,1,0:T(8,128)(2,1)}) %all-gather.9.cloned.1.call-update) | async-done | bytes 4194320 | tf_op jit(solution)/shard_map/all_gather | solution.py:48
  131.7 8.6 %copy.48 = bf16[1,2048,1024]{2,0,1:T(2,128)(2,1)} copy(bf16[1,2048,1024]{2,1,0:T(8,128)(2,1)} %all-gather.9.cloned.1.call-done) | data formatting | bytes 8388608 | tf_op jit(solution)/shard_map/all_gather | solution.py:48
  140.3 0.5 broadcast.121
  140.8 26.0 %reduce.4 = bf16[2048,1024]{1,0:T(8,128)(2,1)} reduce(bf16[2048,1,1024]{2,1,0:T(2,128)(2,1)} %bitcast.63, bf16[]{:T(256)} %broadcast.121), dimensions={1}, to_apply=%bitcast.59.reduce_sub_computation | reduce | bytes 8388610
  166.9 6.2 %reshape.164 = bf16[4,2,262144]{2,1,0:T(2,128)(2,1)} reshape(bf16[2048,1024]{1,0:T(8,128)(2,1)} %reduce.4) | data formatting | bytes 8388608
  173.1 5.0 all-to-all-start.3
  178.6 1.2 reduce-window.6
  180.6 2.9 scatter_custom_fusion
  183.6 1.8 fusion.5
  185.4 1.8 fusion.6
  187.4 5.7 %gather_fusion = bf16[768,4096]{1,0:T(8,128)(2,1)} fusion(bf16[193,4096]{1,0:T(8,128)(2,1)S(1)} %concatenate.3, s32[1024]{0:T(1024)S(1)} %pad_clamp_fusion.1), kind=kCustom, calls=%fused_computation | custom fusion | bytes 12585984 | tf_op jit(solution)/shard_map/gather | solution.py:28
  193.1 33.3 %all-to-all-done.3 = bf16[4,2,262144]{2,1,0:T(2,128)(2,1)} async-done(((bf16[4,2,262144]{2,1,0:T(2,128)(2,1)}), bf16[4,2,262144]{2,1,0:T(2,128)(2,1)}, u32[]{:S(2)}, u32[]{:S(2)}) %all-to-all-start.3) | async-done | bytes 4194336 | tf_op jit(solution)/shard_map/all_to_all | solution.py:50
  226.3 5.3 %all-to-all-start.4 = ((bf16[4,192,4096]{2,1,0:T(8,128)(2,1)}), bf16[4,192,4096]{2,1,0:T(8,128)(2,1)}, u32[]{:S(2)}, u32[]{:S(2)}) async-start(bf16[4,192,4096]{2,1,0:T(8,128)(2,1)} %bitcast.65), calls=%async_computation.4 | async-start | bytes 12582912 | tf_op jit(solution)/shard_map/all_to_all | solution.py:61
  231.7 0.7 all-gather.7.cloned.1.call-update
  232.4 0.5 all-gather.5.cloned.1.call-update
  233.0 0.5 reduce-scatter.2.cloned.1.call-start
  233.5 7.4 %reshape.165 = bf16[2048,1,1024]{2,1,0:T(2,128)(2,1)} reshape(bf16[4,2,262144]{2,1,0:T(2,128)(2,1)} %all-to-all-done.3) | data formatting | bytes 8388608
  240.9 7.9 %copy.40 = bf16[1,2048,1024]{2,1,0:T(8,128)(2,1)} copy(bf16[1,2048,1024]{2,0,1:T(2,128)(2,1)} %bitcast.64) | data formatting | bytes 8388608
  248.9 6.2 %copy.32 = bf16[1,512,4,1024]{1,3,2,0:T(8,128)(2,1)} copy(bf16[1,512,4,1024]{3,1,2,0:T(8,128)(2,1)} %bitcast.66) | data formatting | bytes 8388608 | tf_op jit(solution)/shard_map/all_to_all | solution.py:50
  255.1 35.2 %all-gather.7.cloned.1.call-done = bf16[1,4096,512]{2,1,0:T(8,128)(2,1)} async-done(((bf16[1,2048,512]{2,1,0:T(8,128)(2,1)}), bf16[1,4096,512]{2,1,0:T(8,128)(2,1)}) %all-gather.7.cloned.1.call-update) | async-done | bytes 4194320 | tf_op jit(solution)/shard_map/all_gather | solution.py:47
  290.3 79.5 %all-to-all-done.4 = bf16[4,192,4096]{2,1,0:T(8,128)(2,1)} async-done(((bf16[4,192,4096]{2,1,0:T(8,128)(2,1)}), bf16[4,192,4096]{2,1,0:T(8,128)(2,1)}, u32[]{:S(2)}, u32[]{:S(2)}) %all-to-all-start.4) | async-done | bytes 6291488 | tf_op jit(solution)/shard_map/all_to_all | solution.py:61
  369.8 6.7 %fusion.1 = f32[768,512]{1,0:T(8,128)S(1)} fusion(bf16[768,4096]{1,0:T(8,128)(2,1)} %bitcast.7, bf16[1,4096,512]{2,1,0:T(8,128)(2,1)} %all-gather.7.cloned.1.call-done), kind=kOutput, calls=%fused_computation.5 | convolution fusion | flops 3221225472 | bytes 12058624 | tf_op jit(solution)/shard_map/erd,edf->erf/dot_general | solution.py:63
  376.6 13.5 %fusion = bf16[1,768,4096]{2,1,0:T(8,128)(2,1)} fusion(bf16[512,4096]{0,1:T(8,128)(2,1)} %bitcast.67, f32[768,512]{1,0:T(8,128)S(1)} %fusion.1, bf16[768,4096]{1,0:T(8,128)(2,1)} %bitcast.7, bf16[1,4096,512]{2,1,0:T(8,128)(2,1)} %all-gather.5.cloned.1.call-done), kind=kOutput, calls=%fused_computation.4 | convolution fusion | flops 6448742400 | bytes 22544384 | tf_op jit(solution)/shard_map/erf,efd->erd/dot_general | solution.py:66
  390.1 55.4 %reduce-scatter.2.cloned.1.call-done = bf16[1,768,1024]{2,1,0:T(8,128)(2,1)} async-done(((bf16[1,768,4096]{2,1,0:T(8,128)(2,1)}), bf16[1,768,1024]{2,1,0:T(8,128)(2,1)}) %reduce-scatter.2.cloned.1.call-update) | async-done | bytes 1572880 | tf_op jit(solution)/shard_map/reduce_scatter | solution.py:69
  445.5 1.8 multiply_convert_fusion.2
  447.3 2.4 copy.49
  449.7 11.2 %reduce.5 = bf16[768,1024]{1,0:T(8,128)(2,1)} reduce(bf16[768,1,1024]{2,1,0:T(2,128)(2,1)S(1)} %bitcast.69, bf16[]{:T(256)} %broadcast.121), dimensions={1}, to_apply=%bitcast.60.reduce_sub_computation | reduce | bytes 3145730
  460.9 4.1 reshape.166
  465.1 4.6 all-to-all-start.5
  469.8 6.3 %copy.39 = bf16[1,512,4096]{2,1,0:T(8,128)(2,1)} copy(bf16[1,512,4096]{1,2,0:T(8,128)(2,1)} %bitcast.68) | data formatting | bytes 8388608
  476.2 30.3 %all-to-all-done.5 = bf16[4,2,98304]{2,1,0:T(2,128)(2,1)S(1)} async-done(((bf16[4,2,98304]{2,1,0:T(2,128)(2,1)}), bf16[4,2,98304]{2,1,0:T(2,128)(2,1)S(1)}, u32[]{:S(2)}, u32[]{:S(2)}) %all-to-all-start.5) | async-done | bytes 1572896 | tf_op jit(solution)/shard_map/all_to_all | solution.py:73
  506.4 2.8 reshape.167
  509.2 2.5 copy.47
  511.7 2.1 gather_fusion.1
  513.8 1.0 reshape.134
  514.7 2.8 multiply_reduce_fusion
  517.5 4.6 copy.52
  522.2 2.0 copy.53
  (40 shorter events, 1.8 us)
Async XLA Ops:
  11.0 6.5 %copy-start.5 = (f32[512]{0:T(512)S(1)}, f32[512]{0:T(512)}, u32[]{:S(2)}) copy-start(f32[512]{0:T(512)} %param.10) | copy-start | bytes 6148
  11.0 54.7 %all-to-all-start.2 = ((bf16[4,256,1024]{2,1,0:T(8,128)(2,1)}), bf16[4,256,1024]{2,1,0:T(8,128)(2,1)S(1)}, u32[]{:S(2)}, u32[]{:S(2)}) async-start(bf16[4,256,1024]{2,1,0:T(8,128)(2,1)} %convert_element_type.50), calls=%async_computation.2 | async-start | bytes 4194304 | tf_op jit(solution)/shard_map/all_to_all | solution.py:43
  65.7 1.3 copy-start.1
  67.0 51.3 %all-to-all-start.1 = ((bf16[4,512,512]{2,1,0:T(8,128)(2,1)}), bf16[4,512,512]{2,1,0:T(8,128)(2,1)S(1)}, u32[]{:S(2)}, u32[]{:S(2)}) async-start(bf16[4,512,512]{2,1,0:T(8,128)(2,1)} %get-tuple-element.16), calls=%async_computation.1 | async-start | bytes 4194304 | tf_op jit(solution)/shard_map/all_to_all | solution.py:42
  70.6 61.1 %all-gather.9.cloned.1.call-start = ((), (), s32[]{:S(2)}) async-start(), calls=%async_computation.9 | async-start | bytes 6291456 | tf_op jit(solution)/shard_map/all_gather | solution.py:48
  118.3 22.0 %copy-start = (bf16[4,512,512]{2,1,0:T(8,128)(2,1)}, bf16[4,512,512]{2,1,0:T(8,128)(2,1)S(1)}, u32[]{:S(2)}) copy-start(bf16[4,512,512]{2,1,0:T(8,128)(2,1)S(1)} %all-to-all-done.1) | copy-start | bytes 6291460
  118.3 54.7 %all-to-all-start = ((bf16[4,512,512]{2,1,0:T(8,128)(2,1)}), bf16[4,512,512]{2,1,0:T(8,128)(2,1)}, u32[]{:S(2)}, u32[]{:S(2)}) async-start(bf16[4,512,512]{2,1,0:T(8,128)(2,1)} %get-tuple-element.17), calls=%async_computation | async-start | bytes 4194304 | tf_op jit(solution)/shard_map/all_to_all | solution.py:41
  122.8 60.8 %all-gather.11.cloned.1.call-start = ((), (), s32[]{:S(2)}) async-start(), calls=%async_computation.10 | async-start | bytes 1966080 | tf_op jit(solution)/shard_map/all_gather | solution.py:55
  173.1 5.1 copy-start.3
  173.1 53.3 %all-to-all-start.3 = ((bf16[4,2,262144]{2,1,0:T(2,128)(2,1)}), bf16[4,2,262144]{2,1,0:T(2,128)(2,1)}, u32[]{:S(2)}, u32[]{:S(2)}) async-start(bf16[4,2,262144]{2,1,0:T(2,128)(2,1)} %reshape.164), calls=%async_computation.3 | async-start | bytes 8388608 | tf_op jit(solution)/shard_map/all_to_all | solution.py:50
  226.3 143.4 %all-to-all-start.4 = ((bf16[4,192,4096]{2,1,0:T(8,128)(2,1)}), bf16[4,192,4096]{2,1,0:T(8,128)(2,1)}, u32[]{:S(2)}, u32[]{:S(2)}) async-start(bf16[4,192,4096]{2,1,0:T(8,128)(2,1)} %bitcast.65), calls=%async_computation.4 | async-start | bytes 12582912 | tf_op jit(solution)/shard_map/all_to_all | solution.py:61
  231.7 58.6 %all-gather.7.cloned.1.call-start = ((), (), s32[]{:S(2)}) async-start(), calls=%async_computation.8 | async-start | bytes 6291456 | tf_op jit(solution)/shard_map/all_gather | solution.py:47
  232.4 144.1 %all-gather.5.cloned.1.call-start = ((), (), s32[]{:S(2)}) async-start(), calls=%async_computation.7 | async-start | bytes 6291456 | tf_op jit(solution)/shard_map/all_gather | solution.py:46
  233.0 212.5 %reduce-scatter.2.cloned.1.call-start = ((), (), s32[]{:S(2)}) async-start(), calls=%async_computation.11 | async-start | bytes 7864320 | tf_op jit(solution)/shard_map/reduce_scatter | solution.py:69
  460.9 8.7 %copy-start.4 = (f32[192,2]{0,1:T(2,128)S(1)}, f32[192,2]{0,1:T(2,128)}, u32[]{:S(2)}) copy-start(f32[192,2]{0,1:T(2,128)} %param.9) | copy-start | bytes 4612
  465.1 41.4 %all-to-all-start.5 = ((bf16[4,2,98304]{2,1,0:T(2,128)(2,1)}), bf16[4,2,98304]{2,1,0:T(2,128)(2,1)S(1)}, u32[]{:S(2)}, u32[]{:S(2)}) async-start(bf16[4,2,98304]{2,1,0:T(2,128)(2,1)} %reshape.166), calls=%async_computation.6 | async-start | bytes 3145728 | tf_op jit(solution)/shard_map/all_to_all | solution.py:73
  517.5 4.6 copy-start.2
Sparse Core Ops, SparseCore 0:
  73.5 58.1 all-gather.8
  133.3 19.6 all-gather.10
  234.0 56.2 all-gather.6
  291.7 56.7 all-gather.4
  390.2 55.2 reduce-scatter.1
where the time goes:
time: 540 us; the launch traced here: 531 us
  waiting for transfers between devices  333 us (62%)
  local copies, waits for them, and re-layouts  75.8 us (14%)
  other arithmetic  57.6 us (11%)
  starting transfers between devices  30.2 us (6%)
  matrix products  20.2 us (4%)
  between operations  14.2 us (3%)
    all_to_all x1, waiting for transfers between devices, body(): lax.all_to_all(buffer, 'fs', split_axis=0, concat_axis=1, tiled=True)  79.5 us
    reduce_scatter x1, waiting for transfers between devices, body(): lax.psum_scatter(partial_value.astype(jnp.bfloat16), 'tp', scatter_dimens...  55.4 us
    all_to_all x1, waiting for transfers between devices, body(): lax.all_to_all(up_cast, 'fs', split_axis=0, concat_axis=1, tiled=True)  47 us
    unnamed x23, local copies, waits for them, and re-layouts  45.9 us
    all_to_all x1, waiting for transfers between devices, body(): lax.all_to_all(down_cast, 'fs', split_axis=0, concat_axis=1, tiled=True)  41.4 us
    unnamed x3, other arithmetic  37.3 us
    all_gather x1, waiting for transfers between devices, body(): lax.all_gather(owner_up, 'gr', axis=1, tiled=True)  35.2 us
    all_to_all x1, waiting for transfers between devices, body(): lax.all_to_all(down_full, 'tp', split_axis=1, concat_axis=2, tiled=True)  33.3 us
  transfers between devices with their start and end apart: 11, of which 8 were waited for; matrix products, arithmetic and copies ran while one was open for 18% of the time, Pallas kernels for 0%

commit v1 on v0

--- a/solution.py
+++ b/solution.py
@@ -4,6 +4,18 @@
 from jax.sharding import PartitionSpec as P
 
 EPS = 1e-06
+
+
+def rotated_exchange(x, axis, split, join):
+    ways, here = (lax.axis_size(axis), lax.axis_index(axis))
+    width = x.shape[split] // ways
+    turned = jnp.roll(x, -here * width, axis=split)
+    got = [lax.slice_in_dim(turned, 0, width, axis=split)]
+    for far in range(1, ways):
+        sent = lax.slice_in_dim(turned, far * width, (far + 1) * width, axis=split)
+        got.append(lax.ppermute(sent, axis, [(d, (d + far) % ways) for d in range(ways)]))
+    line = jnp.concatenate(got[::-1], axis=join)
+    return jnp.roll(line, (here + 1) * got[0].shape[join], axis=join)
 
 
 def slot_tables(route_ids, experts, capacity):
@@ -39,7 +51,7 @@
     down_cast = down_master.astype(jnp.bfloat16)
     owner_gate, owner_up, owner_down = (
         lax.all_to_all(gate_cast, "fs", split_axis=0, concat_axis=1, tiled=True),
-        lax.all_to_all(up_cast, "fs", split_axis=0, concat_axis=1, tiled=True),
+        rotated_exchange(up_cast, "fs", 0, 1),
         lax.all_to_all(down_cast, "fs", split_axis=0, concat_axis=1, tiled=True),
     )
     gate_full, up_full, down_full = (

time: 540 us -> 628 us (1.16)
  blocking collectives: 0 us -> 54.4 us
  waiting for transfers between devices: 333 us -> 367 us
    ppermute x0 -> x3, waiting for transfers between devices: none -> 173 us  [rotated_exchange(): lax.ppermute(sent, axis, [(d, (d + far) % ways) for d in range(ways)])]
    all_to_all x2 -> x0, waiting for transfers between devices: 88.4 us -> none  [the longest x1 47 us: body(): lax.all_to_all(up_cast, 'fs', split_axis=0, concat_axis=1, tiled=True)]
    all_to_all x1, waiting for transfers between devices: 79.5 us -> 0.01 us  [body(): lax.all_to_all(buffer, 'fs', split_axis=0, concat_axis=1, tiled=True)]
    all_to_all x0 -> x1, blocking collectives: none -> 54.4 us  [body(): lax.all_to_all(down_cast, 'fs', split_axis=0, concat_axis=1, tiled=True)]
    all_gather x1, waiting for transfers between devices: 8.17 us -> 44.9 us  [body(): lax.all_gather(owner_down, 'gr', axis=1, tiled=True)]
    all_to_all x2 -> x0, starting transfers between devices: 10.1 us -> none  [the longest x1 6.48 us: body(): lax.all_to_all(down_cast, 'fs', split_axis=0, concat_axis=1, tiled=True)]
    all_gather x1, waiting for transfers between devices: 35.2 us -> 25.3 us  [body(): lax.all_gather(owner_up, 'gr', axis=1, tiled=True)]
    unnamed x23 -> x28, local copies, waits for them, and re-layouts: 45.9 us -> 48 us
  transfers between devices with their start and end apart: 11 -> 12, of which waited for: 8 -> 7; matrix products, arithmetic and copies ran while one was open for 18% -> 17% of each run, Pallas kernels for 0% -> 0%
where the time goes in v1:
time: 628 us; the launch traced here: 619 us
  waiting for transfers between devices  367 us (58%)
  local copies, waits for them, and re-layouts  80.6 us (13%)
  other arithmetic  58.6 us (9%)
  blocking collectives  54.4 us (9%)
  starting transfers between devices  24 us (4%)
  matrix products  20.2 us (3%)
  between operations  14.3 us (2%)
    ppermute x3, waiting for transfers between devices, rotated_exchange(): lax.ppermute(sent, axis, [(d, (d + far) % ways) for d in range(ways)])  173 us
    reduce_scatter x1, waiting for transfers between devices, body(): lax.psum_scatter(partial_value.astype(jnp.bfloat16), 'tp', scatter_dimens...  58.1 us
    all_to_all x1, blocking collectives, body(): lax.all_to_all(down_cast, 'fs', split_axis=0, concat_axis=1, tiled=True)  54.4 us
    unnamed x28, local copies, waits for them, and re-layouts  48 us
    all_gather x1, waiting for transfers between devices, body(): lax.all_gather(owner_down, 'gr', axis=1, tiled=True)  44.9 us
    unnamed x3, other arithmetic  37.3 us
    all_to_all x1, waiting for transfers between devices, body(): lax.all_to_all(down_full, 'tp', split_axis=1, concat_axis=2, tiled=True)  33.3 us
    all_to_all x1, waiting for transfers between devices, body(): lax.all_to_all(expert_out, 'fs', split_axis=1, concat_axis=0, tiled=True)  30.3 us
  transfers between devices with their start and end apart: 12, of which 7 were waited for; matrix products, arithmetic and copies ran while one was open for 17% of the time, Pallas kernels for 0%

profile of v1, /device:TPU:0, one launch (start us, length us, event | category | flops | bytes accessed | tf_op | source)
XLA Modules:
  0.0 618.8 jit_solution(10050213905173437280)
XLA Ops:
  7.2 2.5 convert_element_type.50
  9.7 54.4 %all_to_all.60 = bf16[4,256,1024]{2,1,0:T(8,128)(2,1)} all-to-all(bf16[4,256,1024]{2,1,0:T(8,128)(2,1)S(1)} %convert_element_type.50), channel_id=1, replica_groups=mesh['gr'=2,'fs'=4,'tp'=4] {'fs'}, dimensions={0} | all-to-all | bytes 4194304 | tf_op jit(solution)/shard_map/all_to_all | solution.py:55
  64.2 6.8 %multiply_convert_fusion = (bf16[4,512,512]{2,1,0:T(8,128)(2,1)}, bf16[4,512,512]{2,1,0:T(8,128)(2,1)}) fusion(f32[4,512,512]{2,1,0:T(8,128)} %param.12, f32[512]{0:T(512)S(1)} %copy-done.4, f32[4,512,512]{2,1,0:T(8,128)} %param.11), kind=kLoop, calls=%fused_computation.11 | loop fusion | flops 4194304 | bytes 12584960 | tf_op jit(solution)/shard_map/convert_element_type | solution.py:50
  71.0 3.7 all-to-all-start
  74.7 0.7 all-gather.11.cloned.1.call-update
  75.4 44.9 %all-gather.9.cloned.1.call-done = bf16[1,2048,1024]{2,1,0:T(8,128)(2,1)} async-done(((bf16[1,1024,1024]{2,1,0:T(8,128)(2,1)}), bf16[1,2048,1024]{2,1,0:T(8,128)(2,1)}) %all-gather.9.cloned.1.call-update) | async-done | bytes 4194320 | tf_op jit(solution)/shard_map/all_gather | solution.py:60
  120.3 8.6 %copy.48 = bf16[1,2048,1024]{2,0,1:T(2,128)(2,1)} copy(bf16[1,2048,1024]{2,1,0:T(8,128)(2,1)} %all-gather.9.cloned.1.call-done) | data formatting | bytes 8388608 | tf_op jit(solution)/shard_map/all_gather | solution.py:60
  129.4 26.0 %reduce.4 = bf16[2048,1024]{1,0:T(8,128)(2,1)} reduce(bf16[2048,1,1024]{2,1,0:T(2,128)(2,1)} %bitcast.62, bf16[]{:T(256)} %broadcast.127), dimensions={1}, to_apply=%bitcast.58.reduce_sub_computation | reduce | bytes 8388610
  155.5 6.2 %reshape.161 = bf16[4,2,262144]{2,1,0:T(2,128)(2,1)} reshape(bf16[2048,1024]{1,0:T(8,128)(2,1)} %reduce.4) | data formatting | bytes 8388608
  161.7 1.3 copy-done
  163.0 4.9 all-to-all-start.2
  168.4 1.2 reduce-window.6
  170.4 2.9 scatter_custom_fusion
  173.4 1.8 fusion.5
  175.2 1.8 fusion.6
  177.2 5.7 gather_fusion
  182.8 33.3 %all-to-all-done.2 = bf16[4,2,262144]{2,1,0:T(2,128)(2,1)} async-done(((bf16[4,2,262144]{2,1,0:T(2,128)(2,1)}), bf16[4,2,262144]{2,1,0:T(2,128)(2,1)}, u32[]{:S(2)}, u32[]{:S(2)}) %all-to-all-start.2) | async-done | bytes 4194336 | tf_op jit(solution)/shard_map/all_to_all | solution.py:62
  216.1 5.3 all-to-all-start.3
  222.3 2.3 fusion.7
  224.6 1.2 fusion.20
  225.8 3.7 collective-permute-start
  229.5 1.5 collective-permute-start.2
  231.1 104.2 %collective-permute-done = bf16[1,512,512]{2,1,0:T(8,128)(2,1)S(1)} collective-permute-done((bf16[1,512,512]{2,1,0:T(8,128)(2,1)}, bf16[1,512,512]{2,1,0:T(8,128)(2,1)S(1)}, u32[]{:S(2)}, u32[]{:S(2)}) %collective-permute-start) | collective-permute-done | bytes 524320 | tf_op jit(solution)/shard_map/ppermute | solution.py:16
  335.3 69.2 %collective-permute-done.1 = bf16[1,512,512]{2,1,0:T(8,128)(2,1)S(1)} collective-permute-done((bf16[1,512,512]{2,1,0:T(8,128)(2,1)}, bf16[1,512,512]{2,1,0:T(8,128)(2,1)S(1)}, u32[]{:S(2)}, u32[]{:S(2)}) %collective-permute-start.1) | collective-permute-done | bytes 524320 | tf_op jit(solution)/shard_map/ppermute | solution.py:16
  404.5 1.1 constant_dynamic-update-slice_fusion.3
  405.7 1.1 constant_dynamic-update-slice_fusion
  406.8 1.5 constant_dynamic-slice_fusion
  408.3 7.7 %reshape.162 = bf16[2048,1,1024]{2,1,0:T(2,128)(2,1)} reshape(bf16[4,2,262144]{2,1,0:T(2,128)(2,1)} %all-to-all-done.2) | data formatting | bytes 8388608
  416.0 7.5 %copy.40 = bf16[1,2048,1024]{2,1,0:T(8,128)(2,1)} copy(bf16[1,2048,1024]{2,0,1:T(2,128)(2,1)} %bitcast.63) | data formatting | bytes 8388608
  423.5 6.2 copy.32
  429.7 6.7 %fusion.3 = f32[768,512]{1,0:T(8,128)S(1)} fusion(bf16[768,4096]{1,0:T(8,128)(2,1)} %bitcast.6, bf16[1,4096,512]{2,1,0:T(8,128)(2,1)} %all-gather.5.cloned.1.call-done), kind=kOutput, calls=%fused_computation.9 | convolution fusion | flops 3221225472 | bytes 12058624 | tf_op jit(solution)/shard_map/erd,edf->erf/dot_general | solution.py:74
  436.5 25.3 %all-gather.7.cloned.1.call-done = bf16[1,4096,512]{2,1,0:T(8,128)(2,1)} async-done(((bf16[1,2048,512]{2,1,0:T(8,128)(2,1)}), bf16[1,4096,512]{2,1,0:T(8,128)(2,1)}) %all-gather.7.cloned.1.call-update) | async-done | bytes 4194320 | tf_op jit(solution)/shard_map/all_gather | solution.py:59
  461.7 13.5 %fusion = bf16[1,768,4096]{2,1,0:T(8,128)(2,1)} fusion(bf16[512,4096]{0,1:T(8,128)(2,1)} %bitcast.66, f32[768,512]{1,0:T(8,128)S(1)} %fusion.3, bf16[768,4096]{1,0:T(8,128)(2,1)} %bitcast.6, bf16[1,4096,512]{2,1,0:T(8,128)(2,1)} %all-gather.7.cloned.1.call-done), kind=kOutput, calls=%fused_computation.4 | convolution fusion | flops 6448742400 | bytes 22544384 | tf_op jit(solution)/shard_map/erf,efd->erd/dot_general | solution.py:78
  475.2 58.1 %reduce-scatter.2.cloned.1.call-done = bf16[1,768,1024]{2,1,0:T(8,128)(2,1)} async-done(((bf16[1,768,4096]{2,1,0:T(8,128)(2,1)}), bf16[1,768,1024]{2,1,0:T(8,128)(2,1)}) %reduce-scatter.2.cloned.1.call-update) | async-done | bytes 1572880 | tf_op jit(solution)/shard_map/reduce_scatter | solution.py:81
  533.3 1.8 multiply_convert_fusion.2
  535.1 2.4 copy.49
  537.6 11.2 %reduce.5 = bf16[768,1024]{1,0:T(8,128)(2,1)} reduce(bf16[768,1,1024]{2,1,0:T(2,128)(2,1)S(1)} %bitcast.68, bf16[]{:T(256)} %broadcast.127), dimensions={1}, to_apply=%bitcast.59.reduce_sub_computation | reduce | bytes 3145730
  548.8 4.1 reshape.163
  552.9 4.6 all-to-all-start.4
  557.7 6.3 %copy.39 = bf16[1,512,4096]{2,1,0:T(8,128)(2,1)} copy(bf16[1,512,4096]{1,2,0:T(8,128)(2,1)} %bitcast.67) | data formatting | bytes 8388608
  564.0 30.3 %all-to-all-done.4 = bf16[4,2,98304]{2,1,0:T(2,128)(2,1)S(1)} async-done(((bf16[4,2,98304]{2,1,0:T(2,128)(2,1)}), bf16[4,2,98304]{2,1,0:T(2,128)(2,1)S(1)}, u32[]{:S(2)}, u32[]{:S(2)}) %all-to-all-start.4) | async-done | bytes 1572896 | tf_op jit(solution)/shard_map/all_to_all | solution.py:85
  594.3 2.8 reshape.164
  597.0 2.5 copy.47
  599.5 2.1 gather_fusion.1
  601.6 1.0 reshape.131
  602.6 2.8 multiply_reduce_fusion
  605.3 4.6 copy.59
  610.0 2.0 copy.60
  (52 shorter events, 3.3 us)
Async XLA Ops:
  7.2 113.2 %all-gather.9.cloned.1.call-start = ((), (), s32[]{:S(2)}) async-start(), calls=%async_computation.8 | async-start | bytes 6291456 | tf_op jit(solution)/shard_map/all_gather | solution.py:60
  9.7 54.5 %copy-start.4 = (f32[512]{0:T(512)S(1)}, f32[512]{0:T(512)}, u32[]{:S(2)}) copy-start(f32[512]{0:T(512)} %param.10) | copy-start | bytes 6148
  71.0 90.7 %all-to-all-start = ((bf16[4,512,512]{2,1,0:T(8,128)(2,1)}), bf16[4,512,512]{2,1,0:T(8,128)(2,1)S(1)}, u32[]{:S(2)}, u32[]{:S(2)}) async-start(bf16[4,512,512]{2,1,0:T(8,128)(2,1)} %get-tuple-element.20), calls=%async_computation | async-start | bytes 4194304 | tf_op jit(solution)/shard_map/all_to_all | solution.py:53
  74.7 98.7 %all-gather.11.cloned.1.call-start = ((), (), s32[]{:S(2)}) async-start(), calls=%async_computation.9 | async-start | bytes 1966080 | tf_op jit(solution)/shard_map/all_gather | solution.py:67
  161.7 6.2 %copy-start.2 = (s32[192,2]{0,1:T(2,128)S(1)}, s32[192,2]{0,1:T(2,128)}, u32[]{:S(2)}) copy-start(s32[192,2]{0,1:T(2,128)} %param.8) | copy-start | bytes 4612
  161.7 1.3 copy-start
  163.0 53.1 %all-to-all-start.2 = ((bf16[4,2,262144]{2,1,0:T(2,128)(2,1)}), bf16[4,2,262144]{2,1,0:T(2,128)(2,1)}, u32[]{:S(2)}, u32[]{:S(2)}) async-start(bf16[4,2,262144]{2,1,0:T(2,128)(2,1)} %reshape.161), calls=%async_computation.2 | async-start | bytes 8388608 | tf_op jit(solution)/shard_map/all_to_all | solution.py:62
  216.1 213.6 %all-to-all-start.3 = ((bf16[4,192,4096]{2,1,0:T(8,128)(2,1)}), bf16[4,192,4096]{2,1,0:T(8,128)(2,1)}, u32[]{:S(2)}, u32[]{:S(2)}) async-start(bf16[4,192,4096]{2,1,0:T(8,128)(2,1)} %bitcast.64), calls=%async_computation.3 | async-start | bytes 12582912 | tf_op jit(solution)/shard_map/all_to_all | solution.py:73
  221.5 208.3 %all-gather.5.cloned.1.call-start = ((), (), s32[]{:S(2)}) async-start(), calls=%async_computation.6 | async-start | bytes 6291456 | tf_op jit(solution)/shard_map/all_gather | solution.py:58
  222.2 239.5 %all-gather.7.cloned.1.call-start = ((), (), s32[]{:S(2)}) async-start(), calls=%async_computation.7 | async-start | bytes 6291456 | tf_op jit(solution)/shard_map/all_gather | solution.py:59
  225.8 109.4 %collective-permute-start = (bf16[1,512,512]{2,1,0:T(8,128)(2,1)}, bf16[1,512,512]{2,1,0:T(8,128)(2,1)S(1)}, u32[]{:S(2)}, u32[]{:S(2)}) collective-permute-start(bf16[1,512,512]{2,1,0:T(8,128)(2,1)} %get-tuple-element.18), channel_id=1, source_target_pairs={{0,12},{4,0},{8,4},{12,8},{1,13},{5,1},{9,5},{13,9},{2,14},{6,2},{... | collective-permute-start | bytes 1572872 | tf_op jit(solution)/shard_map/ppermute | solution.py:16
  229.5 174.9 %collective-permute-start.1 = (bf16[1,512,512]{2,1,0:T(8,128)(2,1)}, bf16[1,512,512]{2,1,0:T(8,128)(2,1)S(1)}, u32[]{:S(2)}, u32[]{:S(2)}) collective-permute-start(bf16[1,512,512]{2,1,0:T(8,128)(2,1)} %get-tuple-element.17), channel_id=1, source_target_pairs={{0,8},{4,12},{8,0},{12,4},{1,9},{5,13},{9,1},{13,5},{2,10},{6,14},... | collective-permute-start | bytes 1572872 | tf_op jit(solution)/shard_map/ppermute | solution.py:16
  229.5 174.9 %collective-permute-start.2 = (bf16[1,512,512]{2,1,0:T(8,128)(2,1)}, bf16[1,512,512]{2,1,0:T(8,128)(2,1)}, u32[]{:S(2)}, u32[]{:S(2)}) collective-permute-start(bf16[1,512,512]{2,1,0:T(8,128)(2,1)} %get-tuple-element.16), channel_id=1, source_target_pairs={{0,4},{4,8},{8,12},{12,0},{1,5},{5,9},{9,13},{13,1},{2,6},{6,10},{... | collective-permute-start | bytes 1572872 | tf_op jit(solution)/shard_map/ppermute | solution.py:16
  408.3 125.0 %reduce-scatter.2.cloned.1.call-start = ((), (), s32[]{:S(2)}) async-start(), calls=%async_computation.10 | async-start | bytes 7864320 | tf_op jit(solution)/shard_map/reduce_scatter | solution.py:81
  548.8 8.7 %copy-start.3 = (f32[192,2]{0,1:T(2,128)S(1)}, f32[192,2]{0,1:T(2,128)}, u32[]{:S(2)}) copy-start(f32[192,2]{0,1:T(2,128)} %param.9) | copy-start | bytes 4612
  552.9 41.4 %all-to-all-start.4 = ((bf16[4,2,98304]{2,1,0:T(2,128)(2,1)}), bf16[4,2,98304]{2,1,0:T(2,128)(2,1)S(1)}, u32[]{:S(2)}, u32[]{:S(2)}) async-start(bf16[4,2,98304]{2,1,0:T(2,128)(2,1)} %reshape.163), calls=%async_computation.5 | async-start | bytes 3145728 | tf_op jit(solution)/shard_map/all_to_all | solution.py:85
  605.3 4.6 copy-start.1
Sparse Core Ops, SparseCore 0:
  64.3 55.9 all-gather.8
  121.9 19.6 all-gather.10
  223.8 56.2 all-gather.4
  408.4 53.2 all-gather.6
  475.4 57.9 reduce-scatter.1
